TPU v7x, 32 devices: a whole 2x2x4 slice. The times are simulated.
32 devices in a mesh: sp: 8 (over z, x), dp: 4 (over y, core).
Axes of the slice: x: 2, y: 2, z: 4, core: 2. Of those that a mesh axis runs over, the one named last changes fastest.
Arguments:
- stream: bfloat16 [4, 1536, 2048], P('dp', 'sp'), may hold values from -6 to 6
- queries: bfloat16 [4, 1536, 2048], P('dp', 'sp'), may hold values from -6 to 6
- key_rows: bfloat16 [4, 1536, 2048], P('dp', 'sp'), may hold values from -6 to 6
- value_rows: bfloat16 [4, 1536, 4096], P('dp', 'sp'), may hold values from -6 to 6
- input_gate: bfloat16 [4, 1536, 16], P('dp', 'sp'), may hold values from -4 to 206
- forget_gate: bfloat16 [4, 1536, 16], P('dp', 'sp'), may hold values from 0 to 12
- head_gain: float32 [16, 256], P('sp'), may hold values from 0.1 to 1.9
- out_weight: bfloat16 [4096, 2048], P('sp'), may hold values from -0.09375 to 0.09375
- mix_gain: float32 [2048], replicated, may hold values from 0.1 to 1.9
- ffn_gain: float32 [2048], replicated, may hold values from 0.1 to 1.9
- final_gain: float32 [2048], replicated, may hold values from 0.1 to 1.9
- expert_ids: int32 [4, 1536, 4], P('dp', 'sp'), may hold values from 0 to 31, all different within a row; in each aligned block of 192 rows (0 to 191, 192 to 383, ..., all dimensions but the last counted through in order) at most 36 rows name the same one
- route_scores: float32 [4, 1536, 4], P('dp', 'sp'), may hold values from 0.05 to 1
- expert_gate: bfloat16 [32, 2048, 512], P(('sp', 'dp')), may hold values from -0.125 to 0.125
- expert_up: bfloat16 [32, 2048, 512], P(('sp', 'dp')), may hold values from -0.125 to 0.125
- expert_down: bfloat16 [32, 512, 2048], P(('sp', 'dp')), may hold values from -0.25 to 0.25
- shared_gate: bfloat16 [2048, 512], replicated, may hold values from -0.125 to 0.125
- shared_up: bfloat16 [2048, 512], replicated, may hold values from -0.125 to 0.125
- shared_down: bfloat16 [512, 2048], replicated, may hold values from -0.25 to 0.25
Outputs:
- updated: bfloat16 [4, 1536, 2048], P('dp', 'sp')
Inputs may be any that keep to these rules, and one draw needn't show every extreme that they name: `expert_ids`: each token names 4 different experts. Among the tokens of one device no expert is named by more than 36 tokens, a bound that some block reaches of some device.
All inputs are finite; a program needn't handle non-finite values.
Results may differ from a plain program's by a relative error of at most 0.006.
Values may be sent and summed in bfloat16 or wider, within the bound.
No kernel may reach another device: no remote copies, remote signals or barrier semaphores. Data moves between devices by JAX's collectives and lax.ppermute only.
A program may use at most 128 MiB of HBM per device.

v0:
```python
import jax
import jax.numpy as jnp
from jax import lax
from jax.sharding import PartitionSpec as P

BLOCK = 256
EPSILON = 1e-06
ROUTE_BOOST = 2.5
HIGHEST = lax.Precision.HIGHEST


def root_norm(values, gains):
    return values * lax.rsqrt(jnp.mean(values * values, axis=-1, keepdims=True) + EPSILON) * gains


def cell_block(carry, pieces):
    state, normal, stabilizer = carry
    query_part, key_part, value_part, gate_part, decay_part = pieces
    length = query_part.shape[1]
    causal = jnp.tril(jnp.ones((length, length), dtype=bool))
    cumulative = jnp.cumsum(decay_part, axis=-1)
    logits = jnp.where(
        causal[None],
        cumulative[:, :, None] - cumulative[:, None, :] + gate_part[:, None, :],
        -jnp.inf,
    )
    peak = jnp.maximum(cumulative + stabilizer[:, None], jnp.max(logits, axis=-1))
    weights = jnp.exp(logits - peak[:, :, None])
    scores = jnp.einsum("hld,hsd->hls", query_part, key_part, precision=HIGHEST) * weights
    carried = jnp.exp(cumulative + stabilizer[:, None] - peak)
    numerator = jnp.einsum("hls,hsv->hlv", scores, value_part, precision=HIGHEST) + carried[
        :, :, None
    ] * jnp.einsum("hvd,hld->hlv", state, query_part, precision=HIGHEST)
    denominator = jnp.sum(scores, axis=-1) + carried * jnp.einsum(
        "hd,hld->hl", normal, query_part, precision=HIGHEST
    )
    result = numerator / jnp.maximum(jnp.abs(denominator), jnp.exp(-peak))[:, :, None]
    block_end = cumulative[:, -1]
    write_log = block_end[:, None] - cumulative + gate_part
    peak_next = jnp.maximum(block_end + stabilizer, jnp.max(write_log, axis=-1))
    decay_all = jnp.exp(block_end + stabilizer - peak_next)
    written = jnp.exp(write_log - peak_next[:, None])[:, :, None] * key_part
    state = decay_all[:, None, None] * state + jnp.einsum(
        "hlv,hld->hvd", value_part, written, precision=HIGHEST
    )
    normal = decay_all[:, None] * normal + jnp.sum(written, axis=1)
    return ((state, normal, peak_next), result)


def memory_cell(queries, key_rows, value_rows, input_gate, forget_gate):
    length, head_count = (queries.shape[0], queries.shape[1])
    key_width = queries.shape[2]
    value_width = value_rows.shape[2]
    blocks = length // BLOCK

    def to_blocks(tensor):
        shaped = tensor.astype(jnp.float32).reshape((blocks, BLOCK, head_count) + tensor.shape[2:])
        return jnp.moveaxis(shaped, 2, 1)

    decay_log = jax.nn.log_sigmoid(forget_gate.astype(jnp.float32))
    start_state = (
        jnp.zeros((head_count, value_width, key_width), jnp.float32),
        jnp.zeros((head_count, key_width), jnp.float32),
        jnp.zeros((head_count,), jnp.float32),
    )
    pieces = (
        to_blocks(queries),
        to_blocks(key_rows) * key_width ** (-0.5),
        to_blocks(value_rows),
        to_blocks(input_gate),
        to_blocks(decay_log),
    )
    _, outputs = lax.scan(cell_block, start_state, pieces)
    return jnp.moveaxis(outputs, 1, 2).reshape(length, head_count, value_width)


def local(
    stream,
    queries,
    key_rows,
    value_rows,
    input_gate,
    forget_gate,
    head_gain,
    out_weight,
    mix_gain,
    ffn_gain,
    final_gain,
    expert_ids,
    route_scores,
    expert_gate,
    expert_up,
    expert_down,
    shared_gate,
    shared_up,
    shared_down,
):
    token_count = stream.shape[1]
    model_width = stream.shape[2]
    head_count = head_gain.shape[0]
    value_width = head_gain.shape[1]
    head_queries, head_keys, head_values, head_input, head_forget = (
        lax.all_to_all(queries, "sp", split_axis=2, concat_axis=1, tiled=True),
        lax.all_to_all(key_rows, "sp", split_axis=2, concat_axis=1, tiled=True),
        lax.all_to_all(value_rows, "sp", split_axis=2, concat_axis=1, tiled=True),
        lax.all_to_all(input_gate, "sp", split_axis=2, concat_axis=1, tiled=True),
        lax.all_to_all(forget_gate, "sp", split_axis=2, concat_axis=1, tiled=True),
    )
    length = head_input.shape[1]
    cell_out = memory_cell(
        head_queries[0].reshape(length, head_count, -1),
        head_keys[0].reshape(length, head_count, -1),
        head_values[0].reshape(length, head_count, value_width),
        head_input[0],
        head_forget[0],
    )
    normed = (
        root_norm(cell_out, head_gain)
        .astype(jnp.bfloat16)
        .reshape(1, length, head_count * value_width)
    )
    token_rows = lax.all_to_all(normed, "sp", split_axis=1, concat_axis=2, tiled=True)[0]
    mixer_out = jnp.dot(
        token_rows,
        lax.all_gather(out_weight, "sp", axis=0, tiled=True),
        preferred_element_type=jnp.float32,
    )
    residual = stream[0].astype(jnp.float32) + root_norm(mixer_out, mix_gain)
    ffn_input = root_norm(residual, ffn_gain).astype(jnp.bfloat16)
    top_count = expert_ids.shape[2]
    local_count = expert_gate.shape[0]
    expert_count = lax.axis_size("sp") * lax.axis_size("dp") * local_count
    capacity = max(2, 3 * token_count * top_count // (2 * expert_count))
    route_ids = expert_ids[0].reshape(-1)
    chosen = (route_ids[:, None] == jnp.arange(expert_count, dtype=jnp.int32)[None, :]).astype(
        jnp.int32
    )
    before = jnp.sum((jnp.cumsum(chosen, axis=0) - chosen) * chosen, axis=1)
    slot_index = route_ids * capacity + before
    slot_owner = jnp.full((expert_count * capacity,), -1, jnp.int32)
    slot_owner = slot_owner.at[slot_index].set(jnp.arange(token_count * top_count, dtype=jnp.int32))
    filled = slot_owner >= 0
    source = jnp.where(filled, slot_owner // top_count, 0)
    outgoing = jnp.where(filled[:, None], ffn_input[source], jnp.zeros((), jnp.bfloat16))
    outgoing = outgoing.reshape(expert_count, capacity, model_width)
    slot_rows = lax.all_to_all(outgoing, ("sp", "dp"), split_axis=0, concat_axis=0, tiled=True)
    shaped = slot_rows.reshape(-1, local_count, slot_rows.shape[1], model_width)
    gate_proj = jnp.einsum(
        "nlcd,ldf->nlcf", shaped, expert_gate, preferred_element_type=jnp.float32
    )
    up_proj = jnp.einsum("nlcd,ldf->nlcf", shaped, expert_up, preferred_element_type=jnp.float32)
    hidden = (jax.nn.silu(gate_proj) * up_proj).astype(jnp.bfloat16)
    answer = jnp.einsum("nlcf,lfd->nlcd", hidden, expert_down, preferred_element_type=jnp.float32)
    expert_out = answer.astype(jnp.bfloat16).reshape(slot_rows.shape)
    returned = lax.all_to_all(expert_out, ("sp", "dp"), split_axis=0, concat_axis=0, tiled=True)
    answers = returned.reshape(expert_count * capacity, model_width)[slot_index]
    answers = answers.reshape(token_count, top_count, model_width)
    scores = route_scores[0]
    route_share = scores / jnp.sum(scores, axis=1, keepdims=True) * ROUTE_BOOST
    routed = jnp.zeros((token_count, model_width), jnp.float32)
    for column in range(top_count):
        routed = routed + route_share[:, column][:, None] * answers[:, column].astype(jnp.float32)
    shared_hidden = (
        jax.nn.silu(jnp.dot(ffn_input, shared_gate, preferred_element_type=jnp.float32))
        * jnp.dot(ffn_input, shared_up, preferred_element_type=jnp.float32)
    ).astype(jnp.bfloat16)
    shared_out = jnp.dot(shared_hidden, shared_down, preferred_element_type=jnp.float32)
    moe_total = routed + shared_out
    result = (residual + root_norm(moe_total, final_gain)).astype(jnp.bfloat16)
    return result[None]


def solution(mesh):
    placed = (
        P("dp", "sp", None),
        P("dp", "sp", None),
        P("dp", "sp", None),
        P("dp", "sp", None),
        P("dp", "sp", None),
        P("dp", "sp", None),
        P("sp", None),
        P("sp", None),
        P(),
        P(),
        P(),
        P("dp", "sp", None),
        P("dp", "sp", None),
        P(("sp", "dp"), None, None),
        P(("sp", "dp"), None, None),
        P(("sp", "dp"), None, None),
        P(),
        P(),
        P(),
    )
    return jax.shard_map(
        local, mesh=mesh, in_specs=placed, out_specs=P("dp", "sp", None), check_vma=False
    )
```

profile of v0, /device:TPU:0, one launch (start us, length us, event | category | flops | bytes accessed | tf_op | source)
XLA Modules:
  0.0 747.4 jit_solution(1196723427909744174)
XLA Ops:
  9.1 7.3 all-to-all-start
  32.1 12.6 %reduce.11 = bf16[2048,192]{1,0:T(8,128)(2,1)S(1)} reduce(bf16[2048,1,192]{2,1,0:T(2,128)(2,1)} %bitcast.311, bf16[]{:T(256)} %broadcast.272), dimensions={1}, to_apply=%bitcast.222.reduce_sub_computation | reduce | bytes 1572866
  56.6 12.6 %reduce.12 = bf16[2048,192]{1,0:T(8,128)(2,1)S(1)} reduce(bf16[2048,1,192]{2,1,0:T(2,128)(2,1)} %bitcast.312, bf16[]{:T(256)} %broadcast.272), dimensions={1}, to_apply=%bitcast.216.reduce_sub_computation | reduce | bytes 1572866
  77.9 9.9 %copy.82 = bf16[1,192,4096]{1,0,2:T(2,128)(2,1)} copy(bf16[1,192,4096]{2,1,0:T(8,128)(2,1)} %param.24) | data formatting | bytes 3145728 | tf_op args[3]
  87.9 25.0 %reduce.10 = bf16[4096,192]{1,0:T(8,128)(2,1)} reduce(bf16[4096,1,192]{2,1,0:T(2,128)(2,1)} %bitcast.303, bf16[]{:T(256)} %broadcast.272), dimensions={1}, to_apply=%bitcast.214.reduce_sub_computation | reduce | bytes 3145730
  112.8 6.7 reshape.420
  119.5 6.1 all-to-all-start.2
  158.6 38.3 %all-to-all-done.2 = bf16[8,2,49152]{2,1,0:T(2,128)(2,1)} async-done(((bf16[8,2,49152]{2,1,0:T(2,128)(2,1)}), bf16[8,2,49152]{2,1,0:T(2,128)(2,1)}, u32[]{:S(2)}, u32[]{:S(2)}) %all-to-all-start.2) | async-done | bytes 1572896 | tf_op jit(solution)/shard_map/all_to_all | solution.py:105
  196.9 7.2 reshape.421
  204.1 10.8 %copy.83 = f32[1,192,8,512]{3,1,2,0:T(8,128)} copy(bf16[1,192,8,512]{1,0,3,2:T(2,128)(2,1)} %bitcast.302) | data formatting | bytes 4718592 | tf_op jit(solution)/shard_map/transpose | solution.py:58
  220.2 82.9 %while.17 = (s32[]{:T(128)}, f32[2,256,128]{2,1,0:T(8,128)}, f32[2,128]{1,0:T(2,128)S(1)}, f32[2]{0:T(128)S(1)}, f32[6,2,256,256]{3,2,1,0:T(8,128)}, /*index=5*/...) while((s32[]{:T(128)}, f32[2,256,128]{2,1,0:T(8,128)}, ...), condition=%wide.region_7.8_spmd.clone, body=%wide.region_0.7_spmd.clone.sunk | while | flops 1009719296 | bytes 9456510 | solution.py:73
  329.9 14.1 %copy.176 = bf16[1,1536,512]{2,0,1:T(2,128)(2,1)} copy(bf16[1,1536,512]{2,1,0:T(8,128)(2,1)S(1)} %multiply_convert_fusion) | data formatting | bytes 3145728 | tf_op jit(solution)/shard_map/convert_element_type | solution.py:119
  344.0 12.0 %reduce.13 = bf16[1536,512]{1,0:T(8,128)(2,1)} reduce(bf16[1536,1,512]{2,1,0:T(2,128)(2,1)} %bitcast.306, bf16[]{:T(256)} %broadcast.272), dimensions={1}, to_apply=%bitcast.255.reduce_sub_computation | reduce | bytes 3145730
  370.9 28.7 %all-to-all-done.5 = bf16[8,2,49152]{2,1,0:T(2,128)(2,1)} async-done(((bf16[8,2,49152]{2,1,0:T(2,128)(2,1)}), bf16[8,2,49152]{2,1,0:T(2,128)(2,1)}, u32[]{:S(2)}, u32[]{:S(2)}) %all-to-all-start.5) | async-done | bytes 1572896 | tf_op jit(solution)/shard_map/all_to_all | solution.py:122
  399.6 6.7 reshape.431
  410.0 8.2 %multiply_reduce_fusion.3 = (f32[192]{0:T(256)S(1)}, f32[192,2048]{1,0:T(8,128)S(1)}) fusion(bf16[192,4096]{1,0:T(8,128)(2,1)} %bitcast.318, bf16[4096,2048]{1,0:T(8,128)(2,1)} %all-gather.2.cloned.1.call-done), kind=kOutput, calls=%fused_computation.78 | convolution fusion | flops 3222011648 | bytes 19923712 | tf_op jit(solution)/shard_map/dot_general | solution.py:123
  425.8 7.2 gather.9
  436.0 119.3 %all_to_all.70 = bf16[32,36,2048]{2,1,0:T(8,128)(2,1)S(1)} all-to-all(bf16[32,36,2048]{2,1,0:T(8,128)(2,1)S(1)} %broadcast_select_fusion.2), channel_id=1, replica_groups=mesh['sp'=8,'dp'=4] {'sp','dp'}, dimensions={0} | all-to-all | bytes 9437184 | tf_op jit(solution)/shard_map/all_to_all | solution.py:146
  562.1 10.6 %convolution_convert_fusion = bf16[32,36,2048]{2,1,0:T(8,128)(2,1)} fusion(bf16[1,512,2048]{2,1,0:T(8,128)(2,1)S(1)} %copy-done, f32[32,36,512]{2,1,0:T(8,128)} %fusion.24, bf16[32,36,2048]{2,1,0:T(8,128)(2,1)} %copy-done.3, bf16[1,2048,512]{2,1,0:T(8,128)(2,1)} %param.34), kind=kOutput, calls=%fused_computation.49 | convolution fusion | flops 4837736448 | bytes 15990784 | tf_op jit(solution)/shard_map/nlcf,lfd->nlcd/dot_general | solution.py:153
  578.9 114.7 %all-to-all-done.7 = bf16[32,36,2048]{2,1,0:T(8,128)(2,1)} async-done(((bf16[32,36,2048]{2,1,0:T(8,128)(2,1)}), bf16[32,36,2048]{2,1,0:T(8,128)(2,1)}, u32[]{:S(2)}, u32[]{:S(2)}) %all-to-all-start.7) | async-done | bytes 4718624 | tf_op jit(solution)/shard_map/all_to_all | solution.py:155
  693.6 7.2 reshape.370
  700.9 10.0 %gather_fusion.1 = bf16[768,2048]{1,0:T(8,128)(2,1)} fusion(bf16[1152,2048]{1,0:T(8,128)(2,1)} %reshape.370, s32[1024]{0:T(1024)S(1)} %pad_clamp_fusion.1), kind=kCustom, calls=%fused_computation.1 | custom fusion | bytes 6294528 | tf_op jit(solution)/shard_map/gather | solution.py:156
  716.6 12.3 %fusion.64 = (bf16[192,1,2048]{2,1,0:T(2,128)(2,1)}, bf16[192,1,2048]{2,1,0:T(2,128)(2,1)}, bf16[192,1,2048]{2,1,0:T(2,128)(2,1)}, bf16[192,1,2048]{2,1,0:T(2,128)(2,1)}) fusion(bf16[192,4,2048]{2,1,0:T(4,128)(2,1)} %reshape.371), kind=kLoop, calls=%fused_computation.135 | loop fusion | bytes 6291456 | tf_op jit(solution)/shard_map/slice | solution.py:162
  728.9 8.0 %multiply_reduce_fusion.1 = (f32[192]{0:T(256)S(1)}, f32[192,2048]{1,0:T(8,128)}) fusion(bf16[512,2048]{1,0:T(8,128)(2,1)} %param.39, bf16[192,2048]{1,0:T(8,128)(2,1)S(1)} %multiply_convert_fusion.1, bf16[2048,512]{1,0:T(8,128)(2,1)} %param.38, f32[192,512]{1,0:T(8,128)S(1)} %fusion.66, bf16[192,1,2048]{2,1,0:T(2,128)(2,1)} %get-tuple-element.159, ...), kind=kOutput, calls=%fused_computation.75 | convolution fusion | flops 811401024 | bytes 10096384 | tf_op jit(solution)/shard_map/dot_general | solution.py:167
  (268 shorter events, 237.6 us)
Async XLA Ops:
  6.5 555.6 %copy-start = (bf16[1,512,2048]{2,1,0:T(8,128)(2,1)S(1)}, bf16[1,512,2048]{2,1,0:T(8,128)(2,1)}, u32[]{:S(2)}) copy-start(bf16[1,512,2048]{2,1,0:T(8,128)(2,1)} %param.36) | copy-start | bytes 6291460
  9.1 13.8 %all-to-all-start = ((bf16[8,2,192]{2,1,0:T(2,128)(2,1)}), bf16[8,2,192]{2,1,0:T(2,128)(2,1)S(1)}, u32[]{:S(2)}, u32[]{:S(2)}) async-start(bf16[8,2,192]{2,1,0:T(2,128)(2,1)} %reshape.424), calls=%async_computation | async-start | bytes 16384 | tf_op jit(solution)/shard_map/all_to_all | solution.py:107
  22.9 23.9 %all-to-all-start.1 = ((bf16[8,2,192]{2,1,0:T(2,128)(2,1)}), bf16[8,2,192]{2,1,0:T(2,128)(2,1)S(1)}, u32[]{:S(2)}, u32[]{:S(2)}) async-start(bf16[8,2,192]{2,1,0:T(2,128)(2,1)} %reshape.426), calls=%async_computation.1 | async-start | bytes 16384 | tf_op jit(solution)/shard_map/all_to_all | solution.py:106
  46.8 6.1 copy-start.4
  46.8 24.7 %all-to-all-start.3 = ((bf16[8,2,24576]{2,1,0:T(2,128)(2,1)}), bf16[8,2,24576]{2,1,0:T(2,128)(2,1)}, u32[]{:S(2)}, u32[]{:S(2)}) async-start(bf16[8,2,24576]{2,1,0:T(2,128)(2,1)} %reshape.428), calls=%async_computation.3 | async-start | bytes 1572864 | tf_op jit(solution)/shard_map/all_to_all | solution.py:104
  71.5 48.1 %all-to-all-start.4 = ((bf16[8,2,24576]{2,1,0:T(2,128)(2,1)}), bf16[8,2,24576]{2,1,0:T(2,128)(2,1)S(1)}, u32[]{:S(2)}, u32[]{:S(2)}) async-start(bf16[8,2,24576]{2,1,0:T(2,128)(2,1)} %reshape.422), calls=%async_computation.4 | async-start | bytes 1572864 | tf_op jit(solution)/shard_map/all_to_all | solution.py:103
  77.2 332.8 %all-gather.2.cloned.1.call-start = ((), (), s32[]{:S(2)}) async-start(), calls=%async_computation.8 | async-start | bytes 18874368 | tf_op jit(solution)/shard_map/all_gather | solution.py:125
  119.5 6.2 copy-start.10
  119.5 77.4 %all-to-all-start.2 = ((bf16[8,2,49152]{2,1,0:T(2,128)(2,1)}), bf16[8,2,49152]{2,1,0:T(2,128)(2,1)}, u32[]{:S(2)}, u32[]{:S(2)}) async-start(bf16[8,2,49152]{2,1,0:T(2,128)(2,1)} %reshape.420), calls=%async_computation.2 | async-start | bytes 3145728 | tf_op jit(solution)/shard_map/all_to_all | solution.py:105
  360.1 4.4 copy-start.6
  360.1 39.5 %all-to-all-start.5 = ((bf16[8,2,49152]{2,1,0:T(2,128)(2,1)}), bf16[8,2,49152]{2,1,0:T(2,128)(2,1)}, u32[]{:S(2)}, u32[]{:S(2)}) async-start(bf16[8,2,49152]{2,1,0:T(2,128)(2,1)} %reshape.430), calls=%async_computation.5 | async-start | bytes 3145728 | tf_op jit(solution)/shard_map/all_to_all | solution.py:122
  410.0 8.2 %copy-start.2 = (bf16[1,192,2048]{2,1,0:T(8,128)(2,1)S(1)}, bf16[1,192,2048]{2,1,0:T(8,128)(2,1)}, u32[]{:S(2)}) copy-start(bf16[1,192,2048]{2,1,0:T(8,128)(2,1)} %param.21) | copy-start | bytes 2359300
  410.0 8.3 %copy-start.5 = (f32[2048]{0:T(1024)S(1)}, f32[2048]{0:T(1024)}, u32[]{:S(2)}) copy-start(f32[2048]{0:T(1024)} %param.29) | copy-start | bytes 24580
  418.2 1.2 copy-start.1
  418.3 1.1 copy-start.8
  436.0 121.7 %copy-start.11 = (bf16[1,2048,512]{2,1,0:T(8,128)(2,1)S(1)}, bf16[1,2048,512]{2,1,0:T(8,128)(2,1)}, u32[]{:S(2)}) copy-start(bf16[1,2048,512]{2,1,0:T(8,128)(2,1)} %param.35) | copy-start | bytes 6291460
  555.3 2.3 copy-start.3
  572.7 4.0 copy-start.7
  572.7 121.0 %all-to-all-start.7 = ((bf16[32,36,2048]{2,1,0:T(8,128)(2,1)}), bf16[32,36,2048]{2,1,0:T(8,128)(2,1)}, u32[]{:S(2)}, u32[]{:S(2)}) async-start(bf16[32,36,2048]{2,1,0:T(8,128)(2,1)} %convolution_convert_fusion), calls=%async_computation.7 | async-start | bytes 10485760 | tf_op jit(solution)/shard_map/all_to_all | solution.py:155
  728.9 8.0 %copy-start.9 = (f32[2048]{0:T(1024)S(1)}, f32[2048]{0:T(1024)}, u32[]{:S(2)}) copy-start(f32[2048]{0:T(1024)} %param.31) | copy-start | bytes 24580
Sparse Core Ops, SparseCore 0:
  80.1 262.0 all-gather.1
where the time goes:
time: 758 us; the launch traced here: 747 us
  local copies, waits for them, and re-layouts  207 us (27%)
  waiting for transfers between devices  187 us (25%)
  blocking collectives  119 us (16%)
  other arithmetic  94.6 us (12%)
  matrix products  88.1 us (12%)
  starting transfers between devices  37.2 us (5%)
  between operations  14 us (2%)
    all_to_all x1, blocking collectives, local(): lax.all_to_all(outgoing, ('sp', 'dp'), split_axis=0, concat_axis=0, tiled...  119 us
    all_to_all x1, waiting for transfers between devices, local(): lax.all_to_all(expert_out, ('sp', 'dp'), split_axis=0, concat_axis=0, til...  115 us
    unnamed x46, local copies, waits for them, and re-layouts  68.2 us
    unnamed x9, other arithmetic  63.3 us
    all_to_all x1, waiting for transfers between devices, local(): lax.all_to_all(value_rows, 'sp', split_axis=2, concat_axis=1, tiled=True)  38.3 us
    all_to_all x1, waiting for transfers between devices, local(): lax.all_to_all(normed, 'sp', split_axis=1, concat_axis=2, tiled=True)[0]  28.7 us
    transpose x6, local copies, waits for them, and re-layouts, to_blocks(): return jnp.moveaxis(shaped, 2, 1)  25 us
    dot_general x6, matrix products, cell_block(): jnp.einsum('hls,hsv->hlv', scores, value_part, precision=HIGHEST)  18.1 us
  transfers between devices with their start and end apart: 8, of which 5 were waited for; matrix products, arithmetic and copies ran while one was open for 40% of the time, Pallas kernels for 0%

commit v1 on v0

--- a/solution.py
+++ b/solution.py
@@ -1,3 +1,4 @@
+import functools
 import jax
 import jax.numpy as jnp
 from jax import lax
@@ -7,6 +8,19 @@
 EPSILON = 1e-06
 ROUTE_BOOST = 2.5
 HIGHEST = lax.Precision.HIGHEST
+
+
+def guide_object(x_local, pos_dim, dim_no):
+    known = jnp.concatenate(
+        lax.all_to_all(
+            jnp.stack(jnp.split(x_local, lax.psum(1, axis_name="sp"), pos_dim), 0), "sp", 0, 0
+        ),
+        axis=dim_no,
+    )
+    return known
+
+
+recover_the_ladders = functools.partial(guide_object, pos_dim=2, dim_no=1)
 
 
 def root_norm(values, gains):
@@ -102,7 +116,7 @@
     head_queries, head_keys, head_values, head_input, head_forget = (
         lax.all_to_all(queries, "sp", split_axis=2, concat_axis=1, tiled=True),
         lax.all_to_all(key_rows, "sp", split_axis=2, concat_axis=1, tiled=True),
-        lax.all_to_all(value_rows, "sp", split_axis=2, concat_axis=1, tiled=True),
+        recover_the_ladders(value_rows),
         lax.all_to_all(input_gate, "sp", split_axis=2, concat_axis=1, tiled=True),
         lax.all_to_all(forget_gate, "sp", split_axis=2, concat_axis=1, tiled=True),
     )

time: 758 us -> 735 us (0.970)
  waiting for transfers between devices: 187 us -> 212 us
  other arithmetic: 94.6 us -> 70.4 us
  local copies, waits for them, and re-layouts: 207 us -> 185 us
    all_to_all x1, waiting for transfers between devices: 0.01 us -> 31.9 us  [local(): lax.all_to_all(queries, 'sp', split_axis=2, concat_axis=1, tiled=True)]
    unnamed x9 -> x8, other arithmetic: 63.3 us -> 39 us
    unnamed x46 -> x50, local copies, waits for them, and re-layouts: 68.2 us -> 55.8 us
    transpose x6 -> x5, local copies, waits for them, and re-layouts: 25 us -> 13.7 us  [to_blocks(): return jnp.moveaxis(shaped, 2, 1)]
    all_to_all x1, waiting for transfers between devices: 38.3 us -> 29.4 us  [guide_object(): lax.all_to_all(jnp.stack(jnp.split(x_local, lax.psum(1, axis_name='sp'),...]
  transfers between devices with their start and end apart: 8 -> 8, of which waited for: 5 -> 5; matrix products, arithmetic and copies ran while one was open for 40% -> 35% of each run, Pallas kernels for 0% -> 0%
where the time goes in v1:
time: 735 us; the launch traced here: 725 us
  waiting for transfers between devices  212 us (29%)
  local copies, waits for them, and re-layouts  185 us (25%)
  blocking collectives  120 us (16%)
  matrix products  88.1 us (12%)
  other arithmetic  70.4 us (10%)
  starting transfers between devices  35.6 us (5%)
  between operations  14 us (2%)
    all_to_all x1, blocking collectives, local(): lax.all_to_all(outgoing, ('sp', 'dp'), split_axis=0, concat_axis=0, tiled...  120 us
    all_to_all x1, waiting for transfers between devices, local(): lax.all_to_all(expert_out, ('sp', 'dp'), split_axis=0, concat_axis=0, til...  115 us
    unnamed x50, local copies, waits for them, and re-layouts  55.8 us
    unnamed x8, other arithmetic  39 us
    all_to_all x1, waiting for transfers between devices, local(): lax.all_to_all(queries, 'sp', split_axis=2, concat_axis=1, tiled=True)  31.9 us
    all_to_all x1, waiting for transfers between devices, local(): lax.all_to_all(normed, 'sp', split_axis=1, concat_axis=2, tiled=True)[0]  30.8 us
    all_to_all x1, waiting for transfers between devices, guide_object(): lax.all_to_all(jnp.stack(jnp.split(x_local, lax.psum(1, axis_name='sp'),...  29.4 us
    dot_general x6, matrix products, cell_block(): jnp.einsum('hls,hsv->hlv', scores, value_part, precision=HIGHEST)  18.1 us
  transfers between devices with their start and end apart: 8, of which 5 were waited for; matrix products, arithmetic and copies ran while one was open for 35% of the time, Pallas kernels for 0%

profile of v1, /device:TPU:0, one launch (start us, length us, event | category | flops | bytes accessed | tf_op | source)
XLA Modules:
  0.0 724.9 jit_solution(11350512026748193744)
XLA Ops:
  9.3 7.3 %all-to-all-start = ((bf16[8,2,192]{2,1,0:T(2,128)(2,1)}), bf16[8,2,192]{2,1,0:T(2,128)(2,1)S(1)}, u32[]{:S(2)}, u32[]{:S(2)}) async-start(bf16[8,2,192]{2,1,0:T(2,128)(2,1)} %reshape.418), calls=%async_computation | async-start | bytes 16384 | tf_op jit(solution)/shard_map/all_to_all | solution.py:121
  32.4 12.7 %reduce.10 = bf16[2048,192]{1,0:T(8,128)(2,1)S(1)} reduce(bf16[2048,1,192]{2,1,0:T(2,128)(2,1)} %bitcast.319, bf16[]{:T(256)} %broadcast.272), dimensions={1}, to_apply=%bitcast.233.reduce_sub_computation | reduce | bytes 1572866
  47.1 6.1 all-to-all-start.3
  57.7 12.7 %reduce.11 = bf16[2048,192]{1,0:T(8,128)(2,1)S(1)} reduce(bf16[2048,1,192]{2,1,0:T(2,128)(2,1)} %bitcast.320, bf16[]{:T(256)} %broadcast.272), dimensions={1}, to_apply=%bitcast.227.reduce_sub_computation | reduce | bytes 1572866
  75.7 6.0 all-to-all-start.4
  91.4 31.9 %all-to-all-done.4 = bf16[8,2,24576]{2,1,0:T(2,128)(2,1)S(1)} async-done(((bf16[8,2,24576]{2,1,0:T(2,128)(2,1)}), bf16[8,2,24576]{2,1,0:T(2,128)(2,1)S(1)}, u32[]{:S(2)}, u32[]{:S(2)}) %all-to-all-start.4) | async-done | bytes 786464 | tf_op jit(solution)/shard_map/all_to_all | solution.py:117
  151.9 6.0 copy.82
  160.9 29.4 %all-to-all-done.2 = bf16[8,1,192,512]{3,2,1,0:T(8,128)(2,1)} async-done(((bf16[8,1,192,512]{3,2,1,0:T(8,128)(2,1)}), bf16[8,1,192,512]{3,2,1,0:T(8,128)(2,1)}, u32[]{:S(2)}, u32[]{:S(2)}) %all-to-all-start.2) | async-done | bytes 1572896 | tf_op jit(solution)/shard_map/all_to_all | solution.py:15
  194.9 82.9 %while.17 = (s32[]{:T(128)}, f32[2,256,128]{2,1,0:T(8,128)}, f32[2,128]{1,0:T(2,128)S(1)}, f32[2]{0:T(128)S(1)}, f32[6,2,256,256]{3,2,1,0:T(8,128)}, /*index=5*/...) while((s32[]{:T(128)}, f32[2,256,128]{2,1,0:T(8,128)}, ...), condition=%wide.region_7.8_spmd.clone, body=%wide.region_0.7_spmd.clone.sunk | while | flops 1009719296 | bytes 9456510 | solution.py:87
  289.6 6.0 copy.88
  304.8 14.1 %copy.171 = bf16[1,1536,512]{2,0,1:T(2,128)(2,1)} copy(bf16[1,1536,512]{2,1,0:T(8,128)(2,1)S(1)} %multiply_convert_fusion) | data formatting | bytes 3145728 | tf_op jit(solution)/shard_map/convert_element_type | solution.py:133
  318.9 12.2 %reduce.12 = bf16[1536,512]{1,0:T(8,128)(2,1)} reduce(bf16[1536,1,512]{2,1,0:T(2,128)(2,1)} %bitcast.314, bf16[]{:T(256)} %broadcast.272), dimensions={1}, to_apply=%bitcast.266.reduce_sub_computation | reduce | bytes 3145730
  346.0 30.8 %all-to-all-done.5 = bf16[8,2,49152]{2,1,0:T(2,128)(2,1)} async-done(((bf16[8,2,49152]{2,1,0:T(2,128)(2,1)}), bf16[8,2,49152]{2,1,0:T(2,128)(2,1)}, u32[]{:S(2)}, u32[]{:S(2)}) %all-to-all-start.5) | async-done | bytes 1572896 | tf_op jit(solution)/shard_map/all_to_all | solution.py:136
  376.8 6.7 reshape.425
  387.2 8.2 %multiply_reduce_fusion.3 = (f32[192]{0:T(256)S(1)}, f32[192,2048]{1,0:T(8,128)S(1)}) fusion(bf16[192,4096]{1,0:T(8,128)(2,1)} %bitcast.326, bf16[4096,2048]{1,0:T(8,128)(2,1)} %all-gather.2.cloned.1.call-done), kind=kOutput, calls=%fused_computation.78 | convolution fusion | flops 3222011648 | bytes 19923712 | tf_op jit(solution)/shard_map/dot_general | solution.py:137
  397.0 6.0 gather_fusion
  403.0 7.2 gather.9
  413.1 119.6 %all_to_all.66 = bf16[32,36,2048]{2,1,0:T(8,128)(2,1)S(1)} all-to-all(bf16[32,36,2048]{2,1,0:T(8,128)(2,1)S(1)} %broadcast_select_fusion.2), channel_id=1, replica_groups=mesh['sp'=8,'dp'=4] {'sp','dp'}, dimensions={0} | all-to-all | bytes 9437184 | tf_op jit(solution)/shard_map/all_to_all | solution.py:160
  539.6 10.6 %convolution_convert_fusion = bf16[32,36,2048]{2,1,0:T(8,128)(2,1)} fusion(bf16[1,512,2048]{2,1,0:T(8,128)(2,1)S(1)} %copy-done, f32[32,36,512]{2,1,0:T(8,128)} %fusion.24, bf16[32,36,2048]{2,1,0:T(8,128)(2,1)} %copy-done.3, bf16[1,2048,512]{2,1,0:T(8,128)(2,1)} %param.34), kind=kOutput, calls=%fused_computation.49 | convolution fusion | flops 4837736448 | bytes 15990784 | tf_op jit(solution)/shard_map/nlcf,lfd->nlcd/dot_general | solution.py:167
  556.4 114.7 %all-to-all-done.7 = bf16[32,36,2048]{2,1,0:T(8,128)(2,1)} async-done(((bf16[32,36,2048]{2,1,0:T(8,128)(2,1)}), bf16[32,36,2048]{2,1,0:T(8,128)(2,1)}, u32[]{:S(2)}, u32[]{:S(2)}) %all-to-all-start.7) | async-done | bytes 4718624 | tf_op jit(solution)/shard_map/all_to_all | solution.py:169
  671.1 7.2 reshape.367
  678.4 10.0 %gather_fusion.1 = bf16[768,2048]{1,0:T(8,128)(2,1)} fusion(bf16[1152,2048]{1,0:T(8,128)(2,1)} %reshape.367, s32[1024]{0:T(1024)S(1)} %pad_clamp_fusion.1), kind=kCustom, calls=%fused_computation.1 | custom fusion | bytes 6294528 | tf_op jit(solution)/shard_map/gather | solution.py:170
  694.1 12.3 %fusion.64 = (bf16[192,1,2048]{2,1,0:T(2,128)(2,1)}, bf16[192,1,2048]{2,1,0:T(2,128)(2,1)}, bf16[192,1,2048]{2,1,0:T(2,128)(2,1)}, bf16[192,1,2048]{2,1,0:T(2,128)(2,1)}) fusion(bf16[192,4,2048]{2,1,0:T(4,128)(2,1)} %reshape.368), kind=kLoop, calls=%fused_computation.143 | loop fusion | bytes 6291456 | tf_op jit(solution)/shard_map/slice | solution.py:176
  706.5 8.0 %multiply_reduce_fusion.1 = (f32[192]{0:T(256)S(1)}, f32[192,2048]{1,0:T(8,128)}) fusion(bf16[512,2048]{1,0:T(8,128)(2,1)} %param.39, bf16[192,2048]{1,0:T(8,128)(2,1)S(1)} %multiply_convert_fusion.1, bf16[2048,512]{1,0:T(8,128)(2,1)} %param.38, f32[192,512]{1,0:T(8,128)S(1)} %fusion.66, bf16[192,1,2048]{2,1,0:T(2,128)(2,1)} %get-tuple-element.159, ...), kind=kOutput, calls=%fused_computation.75 | convolution fusion | flops 811401024 | bytes 10096384 | tf_op jit(solution)/shard_map/dot_general | solution.py:181
  (271 shorter events, 224.9 us)
Async XLA Ops:
  6.5 533.1 %copy-start = (bf16[1,512,2048]{2,1,0:T(8,128)(2,1)S(1)}, bf16[1,512,2048]{2,1,0:T(8,128)(2,1)}, u32[]{:S(2)}) copy-start(bf16[1,512,2048]{2,1,0:T(8,128)(2,1)} %param.36) | copy-start | bytes 6291460
  9.3 13.8 %all-to-all-start = ((bf16[8,2,192]{2,1,0:T(2,128)(2,1)}), bf16[8,2,192]{2,1,0:T(2,128)(2,1)S(1)}, u32[]{:S(2)}, u32[]{:S(2)}) async-start(bf16[8,2,192]{2,1,0:T(2,128)(2,1)} %reshape.418), calls=%async_computation | async-start | bytes 16384 | tf_op jit(solution)/shard_map/all_to_all | solution.py:121
  23.1 24.0 %all-to-all-start.1 = ((bf16[8,2,192]{2,1,0:T(2,128)(2,1)}), bf16[8,2,192]{2,1,0:T(2,128)(2,1)S(1)}, u32[]{:S(2)}, u32[]{:S(2)}) async-start(bf16[8,2,192]{2,1,0:T(2,128)(2,1)} %reshape.420), calls=%async_computation.1 | async-start | bytes 16384 | tf_op jit(solution)/shard_map/all_to_all | solution.py:120
  47.1 6.8 copy-start.4
  47.1 28.6 %all-to-all-start.3 = ((bf16[8,2,24576]{2,1,0:T(2,128)(2,1)}), bf16[8,2,24576]{2,1,0:T(2,128)(2,1)}, u32[]{:S(2)}, u32[]{:S(2)}) async-start(bf16[8,2,24576]{2,1,0:T(2,128)(2,1)} %reshape.422), calls=%async_computation.3 | async-start | bytes 1572864 | tf_op jit(solution)/shard_map/all_to_all | solution.py:118
  53.2 334.0 %all-gather.2.cloned.1.call-start = ((), (), s32[]{:S(2)}) async-start(), calls=%async_computation.8 | async-start | bytes 18874368 | tf_op jit(solution)/shard_map/all_gather | solution.py:139
  75.7 47.7 %all-to-all-start.4 = ((bf16[8,2,24576]{2,1,0:T(2,128)(2,1)}), bf16[8,2,24576]{2,1,0:T(2,128)(2,1)S(1)}, u32[]{:S(2)}, u32[]{:S(2)}) async-start(bf16[8,2,24576]{2,1,0:T(2,128)(2,1)} %reshape.416), calls=%async_computation.4 | async-start | bytes 1572864 | tf_op jit(solution)/shard_map/all_to_all | solution.py:117
  91.4 36.5 %copy-start.10 = (f32[2,256]{1,0:T(2,128)S(1)}, f32[2,256]{1,0:T(2,128)}, u32[]{:S(2)}) copy-start(f32[2,256]{1,0:T(2,128)} %param.27) | copy-start | bytes 6148
  123.4 66.9 %all-to-all-start.2 = ((bf16[8,1,192,512]{3,2,1,0:T(8,128)(2,1)}), bf16[8,1,192,512]{3,2,1,0:T(8,128)(2,1)}, u32[]{:S(2)}, u32[]{:S(2)}) async-start(bf16[8,1,192,512]{3,2,1,0:T(8,128)(2,1)} %bitcast_dynamic-update-slice_fusion), calls=%async_computation.2 | async-start | bytes 3145728 | tf_op jit(solution)/shard_map/all_to_all | solution.py:15
  335.2 4.4 copy-start.6
  335.2 41.6 %all-to-all-start.5 = ((bf16[8,2,49152]{2,1,0:T(2,128)(2,1)}), bf16[8,2,49152]{2,1,0:T(2,128)(2,1)}, u32[]{:S(2)}, u32[]{:S(2)}) async-start(bf16[8,2,49152]{2,1,0:T(2,128)(2,1)} %reshape.424), calls=%async_computation.5 | async-start | bytes 3145728 | tf_op jit(solution)/shard_map/all_to_all | solution.py:136
  387.2 8.3 %copy-start.2 = (bf16[1,192,2048]{2,1,0:T(8,128)(2,1)S(1)}, bf16[1,192,2048]{2,1,0:T(8,128)(2,1)}, u32[]{:S(2)}) copy-start(bf16[1,192,2048]{2,1,0:T(8,128)(2,1)} %param.21) | copy-start | bytes 2359300
  387.2 8.3 %copy-start.5 = (f32[2048]{0:T(1024)S(1)}, f32[2048]{0:T(1024)}, u32[]{:S(2)}) copy-start(f32[2048]{0:T(1024)} %param.29) | copy-start | bytes 24580
  395.4 1.2 copy-start.1
  395.4 1.1 copy-start.8
  413.1 122.0 %copy-start.11 = (bf16[1,2048,512]{2,1,0:T(8,128)(2,1)S(1)}, bf16[1,2048,512]{2,1,0:T(8,128)(2,1)}, u32[]{:S(2)}) copy-start(bf16[1,2048,512]{2,1,0:T(8,128)(2,1)} %param.35) | copy-start | bytes 6291460
  532.8 2.3 copy-start.3
  550.2 4.0 copy-start.7
  550.2 121.0 %all-to-all-start.7 = ((bf16[32,36,2048]{2,1,0:T(8,128)(2,1)}), bf16[32,36,2048]{2,1,0:T(8,128)(2,1)}, u32[]{:S(2)}, u32[]{:S(2)}) async-start(bf16[32,36,2048]{2,1,0:T(8,128)(2,1)} %convolution_convert_fusion), calls=%async_computation.7 | async-start | bytes 10485760 | tf_op jit(solution)/shard_map/all_to_all | solution.py:169
  706.5 8.0 %copy-start.9 = (f32[2048]{0:T(1024)S(1)}, f32[2048]{0:T(1024)}, u32[]{:S(2)}) copy-start(f32[2048]{0:T(1024)} %param.31) | copy-start | bytes 24580
Sparse Core Ops, SparseCore 0:
  56.1 278.0 all-gather.1
